TPU v7x, 32 devices: a whole 2x2x4 slice. The times are simulated.
32 devices in a mesh: sp: 16 (over z, y, core), tp: 2 (over x).
Axes of the slice: x: 2, y: 2, z: 4, core: 2. Of those that a mesh axis runs over, the one named last changes fastest.
Arguments:
- queries: bfloat16 [16384, 1024], P('sp', 'tp'), may hold values from -8 to 8
- keys: bfloat16 [16384, 256], P('sp', 'tp'), may hold values from -8 to 8
- values: bfloat16 [16384, 256], P('sp', 'tp'), may hold values from -18 to 18
- doc_ids: int32 [16384], P('sp'), may hold values from 0 to 3, never falling along the last dimension, each value on 1 to 8192 neighbouring positions
- sinks: float32 [16], P('tp'), may hold values from 0 to 4
- residual: bfloat16 [16384, 2048], P(('sp', 'tp')), may hold values from -12 to 12
- out_weight: bfloat16 [1024, 2048], P('tp'), may hold values from -0.1875 to 0.1875
- norm_gain: float32 [2048], replicated, may hold values from 0.1 to 1.9
- w_gate: bfloat16 [2048, 5632], P('sp', 'tp'), may hold values from -0.125 to 0.125
- w_value: bfloat16 [2048, 5632], P('sp', 'tp'), may hold values from -0.125 to 0.125
- conv_gate: float32 [3, 5632], P(None, 'tp'), may hold values from -3.5 to 3.5
- conv_value: float32 [3, 5632], P(None, 'tp'), may hold values from -3.5 to 3.5
- w_down: bfloat16 [5632, 2048], P('tp', 'sp'), may hold values from -0.078125 to 0.078125
Outputs:
- layer_out: bfloat16 [16384, 2048], P(('sp', 'tp'))
All inputs are finite; a program needn't handle non-finite values.
Results may differ from a plain program's by a relative error of at most 0.012.
Values may be sent and summed in bfloat16 or wider, within the bound.
A program may use at most 128 MiB of HBM per device.

v0:
```python
import jax
import jax.numpy as jnp
from jax import lax
from jax.sharding import PartitionSpec as P

HEAD_DIM = 64
WINDOW = 128


def shifted(shard, axis, by):
    size = lax.axis_size(axis)
    pairs = [(i, i + by) for i in range(size) if 0 <= i + by < size]
    return lax.ppermute(shard, axis, pairs)


def attend(query_rows, key_ext, value_ext, doc_rows, doc_ext, sinks):
    row_count = query_rows.shape[0]
    block_count = row_count // WINDOW
    kv_heads = key_ext.shape[1] // HEAD_DIM
    group_size = query_rows.shape[1] // (kv_heads * HEAD_DIM)

    def band(t):
        lower = t[:row_count].reshape((block_count, WINDOW) + t.shape[1:])
        upper = t[WINDOW:].reshape((block_count, WINDOW) + t.shape[1:])
        return jnp.concatenate([lower, upper], axis=1)

    query_band = query_rows.reshape(block_count, WINDOW, kv_heads, group_size, HEAD_DIM)
    key_band = band(key_ext).reshape(block_count, 2 * WINDOW, kv_heads, HEAD_DIM)
    value_band = band(value_ext).reshape(block_count, 2 * WINDOW, kv_heads, HEAD_DIM)
    doc_band = band(doc_ext)
    distance = jnp.arange(WINDOW)[:, None] + WINDOW - jnp.arange(2 * WINDOW)[None, :]
    in_window = (distance >= 0) & (distance < WINDOW)
    same_doc = doc_rows.reshape(block_count, WINDOW)[:, :, None] == doc_band[:, None, :]
    keep_mask = in_window[None] & same_doc
    scores = jnp.einsum(
        "nqhgd,nkhd->nhgqk", query_band, key_band, preferred_element_type=jnp.float32
    ) * HEAD_DIM ** (-0.5)
    scores = jnp.where(keep_mask[:, None, None], scores, -jnp.inf)
    sink_logit = sinks.reshape(kv_heads, group_size)[None, :, :, None, None]
    peak = jnp.maximum(jnp.max(scores, axis=-1, keepdims=True), sink_logit)
    expd = jnp.exp(scores - peak)
    probs = (expd / (jnp.sum(expd, axis=-1, keepdims=True) + jnp.exp(sink_logit - peak))).astype(
        jnp.bfloat16
    )
    mixed = jnp.einsum("nhgqk,nkhd->nqhgd", probs, value_band, preferred_element_type=jnp.float32)
    return mixed.astype(jnp.bfloat16).reshape(row_count, -1)


def convolve(ext_rows, doc_ext, taps):
    center = doc_ext[2:]
    same_one = (doc_ext[1:-1] == center)[:, None]
    same_two = (doc_ext[:-2] == center)[:, None]
    ext32 = ext_rows.astype(jnp.float32)
    result = taps[2] * ext32[2:]
    result = result + jnp.where(same_one, taps[1] * ext32[1:-1], 0.0)
    return result + jnp.where(same_two, taps[0] * ext32[:-2], 0.0)


def per_device(
    queries,
    keys,
    values,
    doc_ids,
    sinks,
    residual,
    out_weight,
    norm_gain,
    w_gate,
    w_value,
    conv_gate,
    conv_value,
    w_down,
):
    docs_plus = doc_ids + 1
    prev_keys, prev_values, prev_docs = shifted(
        (keys[-WINDOW:], values[-WINDOW:], docs_plus[-WINDOW:]), "sp", 1
    )
    key_ext = jnp.concatenate([prev_keys, keys], axis=0)
    value_ext = jnp.concatenate([prev_values, values], axis=0)
    doc_ext = jnp.concatenate([prev_docs, docs_plus], axis=0)
    head_out = attend(queries, key_ext, value_ext, docs_plus, doc_ext, sinks)
    head_rows = lax.all_to_all(head_out, "tp", split_axis=0, concat_axis=1, tiled=True)
    proj = jnp.dot(
        head_rows,
        lax.all_gather(out_weight, "tp", axis=0, tiled=True),
        preferred_element_type=jnp.float32,
    )
    mid32 = (residual.astype(jnp.float32) + proj).astype(jnp.bfloat16).astype(jnp.float32)
    normed = (
        mid32 * lax.rsqrt(jnp.mean(mid32 * mid32, axis=-1, keepdims=True) + 1e-06) * norm_gain
    ).astype(jnp.bfloat16)
    whole = lax.all_gather(normed, "tp", axis=0, tiled=True)

    def add_rows(piece):
        return jnp.dot(whole, piece, preferred_element_type=jnp.float32)

    gate_sum = add_rows(lax.all_gather(w_gate, "sp", axis=0, tiled=True))
    value_sum = add_rows(lax.all_gather(w_value, "sp", axis=0, tiled=True))
    gate_pre = gate_sum.astype(jnp.bfloat16)
    value_pre = value_sum.astype(jnp.bfloat16)
    prev_gate, prev_value = shifted((gate_pre[-2:], value_pre[-2:]), "sp", 1)
    conv_docs = jnp.concatenate([prev_docs[-2:], docs_plus], axis=0)
    gate_conv = convolve(jnp.concatenate([prev_gate, gate_pre], axis=0), conv_docs, conv_gate)
    value_conv = convolve(jnp.concatenate([prev_value, value_pre], axis=0), conv_docs, conv_value)
    hidden = (jax.nn.silu(gate_conv) * value_conv).astype(jnp.bfloat16)
    terms = jnp.dot(
        hidden, lax.all_gather(w_down, "sp", axis=1, tiled=True), preferred_element_type=jnp.float32
    )
    sums = lax.psum_scatter(
        terms.astype(jnp.bfloat16), "tp", scatter_dimension=0, tiled=True
    ).astype(jnp.float32)
    return (mid32 + sums).astype(jnp.bfloat16)


def solution(mesh):
    return jax.shard_map(
        per_device,
        mesh=mesh,
        in_specs=(
            P("sp", "tp"),
            P("sp", "tp"),
            P("sp", "tp"),
            P("sp"),
            P("tp"),
            P(("sp", "tp"), None),
            P("tp", None),
            P(),
            P("sp", "tp"),
            P("sp", "tp"),
            P(None, "tp"),
            P(None, "tp"),
            P("tp", "sp"),
        ),
        out_specs=P(("sp", "tp"), None),
        check_vma=False,
    )
```

profile of v0, /device:TPU:0, one launch (start us, length us, event | category | flops | bytes accessed | tf_op | source)
XLA Modules:
  0.0 544.3 jit_solution(59607860426561)
XLA Ops:
  6.5 0.7 broadcast_add_fusion
  7.3 0.5 slice.83
  7.8 2.4 collective-permute-start.1
  10.2 1.4 slice.86
  11.6 4.5 collective-permute-start.2
  16.1 0.8 slice.81
  16.9 1.9 collective-permute-start
  18.9 1.2 reshape.97
  20.1 1.2 reshape.95
  21.3 3.5 reshape.98
  24.9 1.0 copy.36
  25.8 0.7 max.18
  26.6 1.0 copy.32
  27.6 0.3 compare_and_fusion
  28.0 0.2 reshape.96
  28.2 0.4 copy.35
  28.6 1.0 pad_maximum_fusion.1
  29.6 0.2 reshape.94
  29.9 0.4 copy.31
  30.3 2.6 fusion.11
  33.0 2.3 fusion.10
  35.3 0.1 exponential_add_fusion
  35.4 2.4 fusion.25
  37.8 0.7 copy.40
  38.5 0.4 all_to_all.14
  39.0 0.2 copy.41
  39.1 28.8 %all_to_all.19 = bf16[2,512,512]{1,2,0:T(8,128)(2,1)S(1)} all-to-all(bf16[2,512,512]{1,2,0:T(8,128)(2,1)S(1)} %copy.41), channel_id=1, replica_groups=mesh['sp'=16,'tp'=2] {'tp'}, dimensions={0} | all-to-all | bytes 2097152 | tf_op jit(solution)/shard_map/all_to_all | solution.py:82
  67.9 20.5 %all-gather.6.cloned.1.call-done = bf16[1024,2048]{1,0:T(8,128)(2,1)} async-done(((bf16[512,2048]{1,0:T(8,128)(2,1)}), bf16[1024,2048]{1,0:T(8,128)(2,1)}) %all-gather.6.cloned.1.call-update) | async-done | bytes 4194320 | tf_op jit(solution)/shard_map/all_gather | solution.py:85
  88.4 5.6 %fusion.14 = (f32[512]{0:T(512)S(1)}, bf16[512,2048]{1,0:T(8,128)(2,1)S(1)}) fusion(bf16[512,1024]{0,1:T(8,128)(2,1)S(1)} %bitcast.45, bf16[1024,2048]{1,0:T(8,128)(2,1)} %all-gather.6.cloned.1.call-done, bf16[512,2048]{1,0:T(8,128)(2,1)} %param.18), kind=kOutput, calls=%fused_computation.29 | convolution fusion | flops 2153774592 | bytes 9439232 | tf_op jit(solution)/shard_map/dot_general | solution.py:83
  94.1 1.9 fusion.16
  96.0 0.7 all-gather.10.cloned.1.call-update
  96.8 0.5 all-gather.12.cloned.1.call-update
  97.3 0.5 all-gather.14.cloned.1.call-update
  98.0 0.2 slice_reduce_fusion.2
  98.3 54.6 %all-gather.8.cloned.1.call-done = bf16[1024,2048]{1,0:T(8,128)(2,1)} async-done(((bf16[512,2048]{1,0:T(8,128)(2,1)}), bf16[1024,2048]{1,0:T(8,128)(2,1)}) %all-gather.8.cloned.1.call-update) | async-done | bytes 4194320 | tf_op jit(solution)/shard_map/all_gather | solution.py:92
  152.9 96.3 %all-gather.10.cloned.1.call-done = bf16[2048,2816]{1,0:T(8,128)(2,1)} async-done(((bf16[128,2816]{1,0:T(8,128)(2,1)}), bf16[2048,2816]{1,0:T(8,128)(2,1)}) %all-gather.10.cloned.1.call-update) | async-done | bytes 11534352 | tf_op jit(solution)/shard_map/all_gather | solution.py:97
  249.2 17.0 %convolution_convert_fusion.1 = bf16[1024,2816]{1,0:T(8,128)(2,1)S(1)} fusion(bf16[1024,2048]{1,0:T(8,128)(2,1)} %all-gather.8.cloned.1.call-done, bf16[2048,2816]{1,0:T(8,128)(2,1)} %all-gather.10.cloned.1.call-done), kind=kOutput, calls=%fused_computation.28 | convolution fusion | flops 11814043648 | bytes 21495808 | tf_op jit(solution)/shard_map/dot_general | solution.py:95
  266.2 2.5 copy-done
  268.7 2.2 collective-permute-start.3
  270.9 72.8 %all-gather.12.cloned.1.call-done = bf16[2048,2816]{1,0:T(8,128)(2,1)} async-done(((bf16[128,2816]{1,0:T(8,128)(2,1)}), bf16[2048,2816]{1,0:T(8,128)(2,1)}) %all-gather.12.cloned.1.call-update) | async-done | bytes 11534352 | tf_op jit(solution)/shard_map/all_gather | solution.py:98
  343.7 17.1 %convolution_convert_fusion = bf16[1024,2816]{1,0:T(8,128)(2,1)S(1)} fusion(bf16[1024,2048]{1,0:T(8,128)(2,1)} %all-gather.8.cloned.1.call-done, bf16[2048,2816]{1,0:T(8,128)(2,1)} %all-gather.12.cloned.1.call-done), kind=kOutput, calls=%fused_computation.27 | convolution fusion | flops 11814043648 | bytes 21495808 | tf_op jit(solution)/shard_map/dot_general | solution.py:95
  360.9 2.4 collective-permute-start.4
  363.3 5.5 %maximum_convert_fusion = f32[1026,2816]{1,0:T(8,128)} fusion(bf16[1024,2816]{1,0:T(8,128)(2,1)S(1)} %copy-done.1, bf16[2,2816]{1,0:T(2,128)(2,1)S(1)} %collective-permute-done.3), kind=kLoop, calls=%fused_computation.24 | loop fusion | flops 11556864 | bytes 17335296 | tf_op jit(solution)/shard_map/convert_element_type | solution.py:53
  368.7 5.5 %maximum_convert_fusion.1 = f32[1026,2816]{1,0:T(8,128)} fusion(bf16[1024,2816]{1,0:T(8,128)(2,1)S(1)} %convolution_convert_fusion, bf16[2,2816]{1,0:T(2,128)(2,1)S(1)} %collective-permute-done.4), kind=kLoop, calls=%fused_computation.25 | loop fusion | flops 11556864 | bytes 17335296 | tf_op jit(solution)/shard_map/convert_element_type | solution.py:53
  374.2 66.7 %all-gather.14.cloned.1.call-done = bf16[2816,2048]{1,0:T(8,128)(2,1)} async-done(((bf16[2816,128]{1,0:T(8,128)(2,1)}), bf16[2816,2048]{1,0:T(8,128)(2,1)}) %all-gather.14.cloned.1.call-update) | async-done | bytes 11534352 | tf_op jit(solution)/shard_map/all_gather | solution.py:107
  440.9 40.0 %fusion.19 = bf16[1024,2048]{1,0:T(8,128)(2,1)} fusion(bf16[2816,2048]{1,0:T(8,128)(2,1)} %all-gather.14.cloned.1.call-done, f32[1026,2816]{1,0:T(8,128)} %maximum_convert_fusion.1, f32[1026,2816]{1,0:T(8,128)} %maximum_convert_fusion, f32[2816]{0:T(1024)S(1)} %get-tuple-element.9, f32[2816]{0:T(1024)S(1)} %get-tuple-element.10, ...), kind=kOutput, calls=%fused_computation.35 | convolution fusion | flops 11870928896 | bytes 85004288 | tf_op jit(solution)/shard_map/dot_general | solution.py:106
  480.9 52.7 %reduce-scatter.2.cloned.1.call-done = bf16[512,2048]{1,0:T(8,128)(2,1)} async-done(((bf16[1024,2048]{1,0:T(8,128)(2,1)}), bf16[512,2048]{1,0:T(8,128)(2,1)}) %reduce-scatter.2.cloned.1.call-update) | async-done | bytes 2097168 | tf_op jit(solution)/shard_map/reduce_scatter | solution.py:109
  533.6 3.8 fusion.17
  (38 shorter events, 0.6 us)
Async XLA Ops:
  6.5 21.4 %copy-start.2 = (bf16[1024,128]{1,0:T(8,128)(2,1)S(1)}, bf16[1024,128]{1,0:T(8,128)(2,1)}, u32[]{:S(2)}) copy-start(bf16[1024,128]{1,0:T(8,128)(2,1)} %param.14) | copy-start | bytes 786436
  6.5 81.9 %all-gather.6.cloned.1.call-start = ((), (), s32[]{:S(2)}) async-start(), calls=%async_computation.2 | async-start | bytes 6291456 | tf_op jit(solution)/shard_map/all_gather | solution.py:85
  7.8 19.7 %collective-permute-start.1 = (s32[128]{0:T(128)}, s32[128]{0:T(128)S(1)}, u32[]{:S(2)}, u32[]{:S(2)}) collective-permute-start(s32[128]{0:T(128)} %slice.83), channel_id=1, source_target_pairs={{0,2},{2,4},{4,6},{6,8},{8,10},{10,12},{12,14},{14,16},{16,18},{18... | collective-permute-start | bytes 1544 | tf_op jit(solution)/shard_map/ppermute | solution.py:13
  11.6 16.4 %collective-permute-start.2 = (bf16[128,128]{1,0:T(8,128)(2,1)}, bf16[128,128]{1,0:T(8,128)(2,1)S(1)}, u32[]{:S(2)}, u32[]{:S(2)}) collective-permute-start(bf16[128,128]{1,0:T(8,128)(2,1)} %slice.86), channel_id=1, source_target_pairs={{0,2},{2,4},{4,6},{6,8},{8,10},{10,12},{12,14},{14,16},{16,18},{18... | collective-permute-start | bytes 98312 | tf_op jit(solution)/shard_map/ppermute | solution.py:13
  16.9 11.7 %collective-permute-start = (bf16[128,128]{1,0:T(8,128)(2,1)S(1)}, bf16[128,128]{1,0:T(8,128)(2,1)S(1)}, u32[]{:S(2)}, u32[]{:S(2)}) collective-permute-start(bf16[128,128]{1,0:T(8,128)(2,1)S(1)} %slice.81), channel_id=1, source_target_pairs={{0,2},{2,4},{4,6},{6,8},{8,10},{10,12},{12,14},{14,16},{16,18},{18... | collective-permute-start | bytes 98312 | tf_op jit(solution)/shard_map/ppermute | solution.py:13
  18.8 134.1 %all-gather.8.cloned.1.call-start = ((), (), s32[]{:S(2)}) async-start(), calls=%async_computation.3 | async-start | bytes 6291456 | tf_op jit(solution)/shard_map/all_gather | solution.py:92
  30.3 5.1 copy-start.3
  39.0 55.1 %copy-start.6 = (f32[2048]{0:T(1024)S(1)}, f32[2048]{0:T(1024)}, u32[]{:S(2)}) copy-start(f32[2048]{0:T(1024)} %param.20) | copy-start | bytes 24580
  88.4 9.5 %copy-start.4 = (f32[3,2816]{1,0:T(4,128)S(1)}, f32[3,2816]{1,0:T(4,128)}, u32[]{:S(2)}) copy-start(f32[3,2816]{1,0:T(4,128)} %param.24) | copy-start | bytes 101380
  88.4 9.5 %copy-start.5 = (f32[3,2816]{1,0:T(4,128)S(1)}, f32[3,2816]{1,0:T(4,128)}, u32[]{:S(2)}) copy-start(f32[3,2816]{1,0:T(4,128)} %param.23) | copy-start | bytes 101380
  96.0 153.2 %all-gather.10.cloned.1.call-start = ((), (), s32[]{:S(2)}) async-start(), calls=%async_computation.4 | async-start | bytes 12255232 | tf_op jit(solution)/shard_map/all_gather | solution.py:97
  96.7 247.0 %all-gather.12.cloned.1.call-start = ((), (), s32[]{:S(2)}) async-start(), calls=%async_computation.5 | async-start | bytes 12255232 | tf_op jit(solution)/shard_map/all_gather | solution.py:98
  97.3 343.6 %all-gather.14.cloned.1.call-start = ((), (), s32[]{:S(2)}) async-start(), calls=%async_computation.6 | async-start | bytes 12255232 | tf_op jit(solution)/shard_map/all_gather | solution.py:107
  97.9 435.7 %reduce-scatter.2.cloned.1.call-start = ((), (), s32[]{:S(2)}) async-start(), calls=%async_computation.7 | async-start | bytes 6291456 | tf_op jit(solution)/shard_map/reduce_scatter | solution.py:109
  266.2 2.5 copy-start
  268.7 94.5 %collective-permute-start.3 = (bf16[2,2816]{1,0:T(2,128)(2,1)S(1)}, bf16[2,2816]{1,0:T(2,128)(2,1)S(1)}, u32[]{:S(2)}, u32[]{:S(2)}) collective-permute-start(bf16[2,2816]{1,0:T(2,128)(2,1)S(1)} %slice.105), channel_id=1, source_target_pairs={{0,2},{2,4},{4,6},{6,8},{8,10},{10,12},{12,14},{14,16},{16,18},{18... | collective-permute-start | bytes 33800 | tf_op jit(solution)/shard_map/ppermute | solution.py:13
  343.7 19.6 %copy-start.1 = (bf16[1024,2816]{1,0:T(8,128)(2,1)S(1)}, bf16[1024,2816]{1,0:T(8,128)(2,1)}, u32[]{:S(2)}) copy-start(bf16[1024,2816]{1,0:T(8,128)(2,1)} %copy-done) | copy-start | bytes 17301508
  360.9 7.9 %collective-permute-start.4 = (bf16[2,2816]{1,0:T(2,128)(2,1)S(1)}, bf16[2,2816]{1,0:T(2,128)(2,1)S(1)}, u32[]{:S(2)}, u32[]{:S(2)}) collective-permute-start(bf16[2,2816]{1,0:T(2,128)(2,1)S(1)} %slice.111), channel_id=1, source_target_pairs={{0,2},{2,4},{4,6},{6,8},{8,10},{10,12},{12,14},{14,16},{16,18},{18... | collective-permute-start | bytes 33800 | tf_op jit(solution)/shard_map/ppermute | solution.py:13
Sparse Core Ops, SparseCore 0:
  18.9 69.4 all-gather.5
  96.1 56.7 all-gather.7
  155.1 93.9 all-gather.9
  251.3 92.3 all-gather.11
  345.7 95.1 all-gather.13
  481.0 52.5 reduce-scatter.1
where the time goes:
time: 545 us; the launch traced here: 544 us
  waiting for transfers between devices  365 us (67%)
  matrix products  84.8 us (16%)
  blocking collectives  28.8 us (5%)
  other arithmetic  21.3 us (4%)
  local copies, waits for them, and re-layouts  16.6 us (3%)
  between operations  13.8 us (3%)
  starting transfers between devices  13.5 us (2%)
    all_gather x1, waiting for transfers between devices, per_device(): gate_sum = add_rows(lax.all_gather(w_gate, 'sp', axis=0, tiled=True))  96.3 us
    all_gather x1, waiting for transfers between devices, per_device(): value_sum = add_rows(lax.all_gather(w_value, 'sp', axis=0, tiled=True))  72.8 us
    all_gather x1, waiting for transfers between devices, per_device(): lax.all_gather(w_down, 'sp', axis=1, tiled=True)  66.7 us
    all_gather x1, waiting for transfers between devices, per_device(): whole = lax.all_gather(normed, 'tp', axis=0, tiled=True)  54.6 us
    reduce_scatter x1, waiting for transfers between devices, per_device(): lax.psum_scatter(terms.astype(jnp.bfloat16), 'tp', scatter_dimension=0, t...  52.7 us
    dot_general x1, matrix products, per_device(): jnp.dot(hidden, lax.all_gather(w_down, 'sp', axis=1, tiled=True), preferr...  40 us
    dot_general x2, matrix products, add_rows(): return jnp.dot(whole, piece, preferred_element_type=jnp.float32)  34.2 us
    all_to_all x1, blocking collectives, per_device(): lax.all_to_all(head_out, 'tp', split_axis=0, concat_axis=1, tiled=True)  28.8 us
  transfers between devices with their start and end apart: 11, of which 6 were waited for; matrix products, arithmetic and copies ran while one was open for 12% of the time, Pallas kernels for 0%

commit v1 on v0

--- a/solution.py
+++ b/solution.py
@@ -104,7 +104,9 @@
     value_conv = convolve(jnp.concatenate([prev_value, value_pre], axis=0), conv_docs, conv_value)
     hidden = (jax.nn.silu(gate_conv) * value_conv).astype(jnp.bfloat16)
     terms = jnp.dot(
-        hidden, lax.all_gather(w_down, "sp", axis=1, tiled=True), preferred_element_type=jnp.float32
+        hidden,
+        jnp.concatenate(jax.lax.all_gather(w_down, "sp"), 1),
+        preferred_element_type=jnp.float32,
     )
     sums = lax.psum_scatter(
         terms.astype(jnp.bfloat16), "tp", scatter_dimension=0, tiled=True

time: 545 us -> 581 us (1.066)
  local copies, waits for them, and re-layouts: 16.6 us -> 32.6 us
  waiting for transfers between devices: 365 us -> 376 us
  matrix products: 84.8 us -> 91.7 us
    all_gather x1, waiting for transfers between devices: 72.8 us -> 96.3 us  [per_device(): value_sum = add_rows(lax.all_gather(w_value, 'sp', axis=0, tiled=True))]
    all_gather x1, waiting for transfers between devices: 96.3 us -> 72.8 us  [per_device(): gate_sum = add_rows(lax.all_gather(w_gate, 'sp', axis=0, tiled=True))]
    reshape x0 -> x1, local copies, waits for them, and re-layouts: none -> 15 us  [per_device(): jnp.concatenate(jax.lax.all_gather(w_down, 'sp'), 1)]
    all_gather x1, waiting for transfers between devices: 66.7 us -> 75.9 us  [per_device(): jax.lax.all_gather(w_down, 'sp')]
  transfers between devices with their start and end apart: 11 -> 11, of which waited for: 6 -> 6; matrix products, arithmetic and copies ran while one was open for 12% -> 14% of each run, Pallas kernels for 0% -> 0%
where the time goes in v1:
time: 581 us; the launch traced here: 580 us
  waiting for transfers between devices  376 us (65%)
  matrix products  91.7 us (16%)
  local copies, waits for them, and re-layouts  32.6 us (6%)
  blocking collectives  28.8 us (5%)
  other arithmetic  23.8 us (4%)
  between operations  13.8 us (2%)
  starting transfers between devices  13.7 us (2%)
    all_gather x1, waiting for transfers between devices, per_device(): value_sum = add_rows(lax.all_gather(w_value, 'sp', axis=0, tiled=True))  96.3 us
    all_gather x1, waiting for transfers between devices, per_device(): jax.lax.all_gather(w_down, 'sp')  75.9 us
    all_gather x1, waiting for transfers between devices, per_device(): gate_sum = add_rows(lax.all_gather(w_gate, 'sp', axis=0, tiled=True))  72.8 us
    all_gather x1, waiting for transfers between devices, per_device(): whole = lax.all_gather(normed, 'tp', axis=0, tiled=True)  54.6 us
    reduce_scatter x1, waiting for transfers between devices, per_device(): lax.psum_scatter(terms.astype(jnp.bfloat16), 'tp', scatter_dimension=0, t...  53.8 us
    dot_general x1, matrix products, per_device(): jnp.dot(hidden, jnp.concatenate(jax.lax.all_gather(w_down, 'sp'), 1), pre...  45.5 us
    dot_general x2, matrix products, add_rows(): return jnp.dot(whole, piece, preferred_element_type=jnp.float32)  35.5 us
    all_to_all x1, blocking collectives, per_device(): lax.all_to_all(head_out, 'tp', split_axis=0, concat_axis=1, tiled=True)  28.8 us
  transfers between devices with their start and end apart: 11, of which 6 were waited for; matrix products, arithmetic and copies ran while one was open for 14% of the time, Pallas kernels for 0%

profile of v1, /device:TPU:0, one launch (start us, length us, event | category | flops | bytes accessed | tf_op | source)
XLA Modules:
  0.0 580.0 jit_solution(3146788316016367210)
XLA Ops:
  6.5 0.7 broadcast_add_fusion
  7.3 0.6 slice.83
  7.8 2.4 collective-permute-start.1
  10.2 1.4 slice.86
  11.6 4.5 collective-permute-start.2
  16.1 0.8 slice.81
  16.9 1.9 collective-permute-start
  18.9 1.2 reshape.106
  20.1 1.2 reshape.104
  21.4 3.5 reshape.107
  24.9 1.0 copy.50
  25.9 0.7 max.18
  26.6 1.0 copy.46
  27.6 0.3 compare_and_fusion
  28.0 0.2 reshape.105
  28.3 0.4 copy.49
  28.6 1.0 pad_maximum_fusion.1
  29.7 0.2 reshape.103
  29.9 0.4 copy.45
  30.3 2.6 fusion.11
  33.0 2.3 fusion.10
  35.4 2.4 fusion.25
  37.9 0.7 copy.54
  38.5 0.4 all_to_all.14
  39.2 28.8 %all_to_all.19 = bf16[2,512,512]{1,2,0:T(8,128)(2,1)S(1)} all-to-all(bf16[2,512,512]{1,2,0:T(8,128)(2,1)S(1)} %copy.55), channel_id=1, replica_groups=mesh['sp'=16,'tp'=2] {'tp'}, dimensions={0} | all-to-all | bytes 2097152 | tf_op jit(solution)/shard_map/all_to_all | solution.py:82
  68.0 20.5 %all-gather.7.cloned.1.call-done = bf16[1024,2048]{1,0:T(8,128)(2,1)} async-done(((bf16[512,2048]{1,0:T(8,128)(2,1)}), bf16[1024,2048]{1,0:T(8,128)(2,1)}) %all-gather.7.cloned.1.call-update) | async-done | bytes 4194320 | tf_op jit(solution)/shard_map/all_gather | solution.py:85
  88.5 5.6 fusion.14
  94.1 1.9 fusion.16
  96.1 0.7 all-gather.13.cloned.1.call-update
  96.8 0.5 all-gather.11.cloned.1.call-update
  97.4 0.5 all-gather.15.cloned.1.call-update
  98.0 0.2 slice_reduce_fusion.2
  98.3 54.6 %all-gather.9.cloned.1.call-done = bf16[1024,2048]{1,0:T(8,128)(2,1)} async-done(((bf16[512,2048]{1,0:T(8,128)(2,1)}), bf16[1024,2048]{1,0:T(8,128)(2,1)}) %all-gather.9.cloned.1.call-update) | async-done | bytes 4194320 | tf_op jit(solution)/shard_map/all_gather | solution.py:92
  152.9 96.3 %all-gather.13.cloned.1.call-done = bf16[2048,2816]{1,0:T(8,128)(2,1)} async-done(((bf16[128,2816]{1,0:T(8,128)(2,1)}), bf16[2048,2816]{1,0:T(8,128)(2,1)}) %all-gather.13.cloned.1.call-update) | async-done | bytes 11534352 | tf_op jit(solution)/shard_map/all_gather | solution.py:98
  249.2 17.0 %convolution_convert_fusion = bf16[1024,2816]{1,0:T(8,128)(2,1)S(1)} fusion(bf16[1024,2048]{1,0:T(8,128)(2,1)} %all-gather.9.cloned.1.call-done, bf16[2048,2816]{1,0:T(8,128)(2,1)} %all-gather.13.cloned.1.call-done), kind=kOutput, calls=%fused_computation.27 | convolution fusion | flops 11814043648 | bytes 21495808 | tf_op jit(solution)/shard_map/dot_general | solution.py:95
  266.2 2.5 copy-done
  268.7 2.2 collective-permute-start.4
  270.9 72.8 %all-gather.11.cloned.1.call-done = bf16[2048,2816]{1,0:T(8,128)(2,1)} async-done(((bf16[128,2816]{1,0:T(8,128)(2,1)}), bf16[2048,2816]{1,0:T(8,128)(2,1)}) %all-gather.11.cloned.1.call-update) | async-done | bytes 11534352 | tf_op jit(solution)/shard_map/all_gather | solution.py:97
  343.7 18.5 %convolution_convert_fusion.1 = bf16[1024,2816]{1,0:T(8,128)(2,1)} fusion(bf16[1024,2048]{1,0:T(8,128)(2,1)} %all-gather.9.cloned.1.call-done, bf16[2048,2816]{1,0:T(8,128)(2,1)} %all-gather.11.cloned.1.call-done), kind=kOutput, calls=%fused_computation.28 | convolution fusion | flops 11814043648 | bytes 21495808 | tf_op jit(solution)/shard_map/dot_general | solution.py:95
  362.2 75.9 %all-gather.15.cloned.1.call-done = bf16[45056,128]{1,0:T(8,128)(2,1)} async-done(((bf16[2816,128]{1,0:T(8,128)(2,1)}), bf16[45056,128]{1,0:T(8,128)(2,1)}) %all-gather.15.cloned.1.call-update) | async-done | bytes 11534352 | tf_op jit(solution)/shard_map/all_gather | solution.py:108
  438.1 15.0 %copy.56 = bf16[2816,16,128]{0,2,1:T(8,128)(2,1)} copy(bf16[2816,16,128]{2,0,1:T(8,128)(2,1)} %bitcast.49) | data formatting | bytes 23068672 | tf_op jit(solution)/shard_map/reshape | solution.py:108
  453.1 1.0 slice.105
  454.1 2.5 collective-permute-start.3
  456.6 8.1 %maximum_convert_fusion.1 = f32[1026,2816]{1,0:T(8,128)} fusion(bf16[1024,2816]{1,0:T(8,128)(2,1)} %copy-done, bf16[2,2816]{1,0:T(2,128)(2,1)S(1)} %collective-permute-done.4), kind=kLoop, calls=%fused_computation.25 | loop fusion | flops 11556864 | bytes 17335296 | tf_op jit(solution)/shard_map/convert_element_type | solution.py:53
  464.8 5.4 maximum_convert_fusion
  470.1 45.5 %fusion.19 = bf16[1024,2048]{1,0:T(8,128)(2,1)} fusion(bf16[2816,2048]{0,1:T(8,128)(2,1)} %bitcast.50, f32[1026,2816]{1,0:T(8,128)} %maximum_convert_fusion.1, f32[1026,2816]{1,0:T(8,128)} %maximum_convert_fusion, f32[2816]{0:T(1024)S(1)} %get-tuple-element.9, f32[2816]{0:T(1024)S(1)} %get-tuple-element.10, f32[2816]{0:T(1024)S(1)} %get-tuple-element.8, ...), kind=kOutput, calls=%fused_computation.35 | convolution fusion | flops 11870928896 | bytes 85004288 | tf_op jit(solution)/shard_map/dot_general | solution.py:106
  515.7 53.8 %reduce-scatter.2.cloned.1.call-done = bf16[512,2048]{1,0:T(8,128)(2,1)} async-done(((bf16[1024,2048]{1,0:T(8,128)(2,1)}), bf16[512,2048]{1,0:T(8,128)(2,1)}) %reduce-scatter.2.cloned.1.call-update) | async-done | bytes 2097168 | tf_op jit(solution)/shard_map/reduce_scatter | solution.py:111
  569.4 3.7 fusion.17
  (42 shorter events, 0.9 us)
Async XLA Ops:
  6.5 21.5 %copy-start.1 = (bf16[1024,128]{1,0:T(8,128)(2,1)S(1)}, bf16[1024,128]{1,0:T(8,128)(2,1)}, u32[]{:S(2)}) copy-start(bf16[1024,128]{1,0:T(8,128)(2,1)} %param.14) | copy-start | bytes 786436
  6.5 81.9 %all-gather.7.cloned.1.call-start = ((), (), s32[]{:S(2)}) async-start(), calls=%async_computation.2 | async-start | bytes 6291456 | tf_op jit(solution)/shard_map/all_gather | solution.py:85
  7.8 19.8 %collective-permute-start.1 = (s32[128]{0:T(128)}, s32[128]{0:T(128)S(1)}, u32[]{:S(2)}, u32[]{:S(2)}) collective-permute-start(s32[128]{0:T(128)} %slice.83), channel_id=1, source_target_pairs={{0,2},{2,4},{4,6},{6,8},{8,10},{10,12},{12,14},{14,16},{16,18},{18... | collective-permute-start | bytes 1544 | tf_op jit(solution)/shard_map/ppermute | solution.py:13
  11.6 16.4 %collective-permute-start.2 = (bf16[128,128]{1,0:T(8,128)(2,1)}, bf16[128,128]{1,0:T(8,128)(2,1)S(1)}, u32[]{:S(2)}, u32[]{:S(2)}) collective-permute-start(bf16[128,128]{1,0:T(8,128)(2,1)} %slice.86), channel_id=1, source_target_pairs={{0,2},{2,4},{4,6},{6,8},{8,10},{10,12},{12,14},{14,16},{16,18},{18... | collective-permute-start | bytes 98312 | tf_op jit(solution)/shard_map/ppermute | solution.py:13
  16.9 11.7 %collective-permute-start = (bf16[128,128]{1,0:T(8,128)(2,1)S(1)}, bf16[128,128]{1,0:T(8,128)(2,1)S(1)}, u32[]{:S(2)}, u32[]{:S(2)}) collective-permute-start(bf16[128,128]{1,0:T(8,128)(2,1)S(1)} %slice.81), channel_id=1, source_target_pairs={{0,2},{2,4},{4,6},{6,8},{8,10},{10,12},{12,14},{14,16},{16,18},{18... | collective-permute-start | bytes 98312 | tf_op jit(solution)/shard_map/ppermute | solution.py:13
  18.8 134.1 %all-gather.9.cloned.1.call-start = ((), (), s32[]{:S(2)}) async-start(), calls=%async_computation.3 | async-start | bytes 6291456 | tf_op jit(solution)/shard_map/all_gather | solution.py:92
  30.3 5.1 copy-start.2
  39.0 55.1 %copy-start.5 = (f32[2048]{0:T(1024)S(1)}, f32[2048]{0:T(1024)}, u32[]{:S(2)}) copy-start(f32[2048]{0:T(1024)} %param.20) | copy-start | bytes 24580
  88.5 9.5 %copy-start.3 = (f32[3,2816]{1,0:T(4,128)S(1)}, f32[3,2816]{1,0:T(4,128)}, u32[]{:S(2)}) copy-start(f32[3,2816]{1,0:T(4,128)} %param.24) | copy-start | bytes 101380
  88.5 9.5 %copy-start.4 = (f32[3,2816]{1,0:T(4,128)S(1)}, f32[3,2816]{1,0:T(4,128)}, u32[]{:S(2)}) copy-start(f32[3,2816]{1,0:T(4,128)} %param.23) | copy-start | bytes 101380
  96.0 153.2 %all-gather.13.cloned.1.call-start = ((), (), s32[]{:S(2)}) async-start(), calls=%async_computation.5 | async-start | bytes 12255232 | tf_op jit(solution)/shard_map/all_gather | solution.py:98
  96.8 247.0 %all-gather.11.cloned.1.call-start = ((), (), s32[]{:S(2)}) async-start(), calls=%async_computation.4 | async-start | bytes 12255232 | tf_op jit(solution)/shard_map/all_gather | solution.py:97
  97.3 340.8 %all-gather.15.cloned.1.call-start = ((), (), s32[]{:S(2)}) async-start(), calls=%async_computation.7 | async-start | bytes 12255232 | tf_op jit(solution)/shard_map/all_gather | solution.py:108
  97.9 471.5 %reduce-scatter.2.cloned.1.call-start = ((), (), s32[]{:S(2)}) async-start(), calls=%async_computation.6 | async-start | bytes 6291456 | tf_op jit(solution)/shard_map/reduce_scatter | solution.py:111
  266.2 2.5 copy-start
  268.7 187.9 %collective-permute-start.4 = (bf16[2,2816]{1,0:T(2,128)(2,1)S(1)}, bf16[2,2816]{1,0:T(2,128)(2,1)S(1)}, u32[]{:S(2)}, u32[]{:S(2)}) collective-permute-start(bf16[2,2816]{1,0:T(2,128)(2,1)S(1)} %slice.111), channel_id=1, source_target_pairs={{0,2},{2,4},{4,6},{6,8},{8,10},{10,12},{12,14},{14,16},{16,18},{18... | collective-permute-start | bytes 33800 | tf_op jit(solution)/shard_map/ppermute | solution.py:13
  453.1 11.6 %slice-start = ((s8[5767168]{0:T(1024)(128)(4,1)}), s8[4194304]{0:T(1024)(128)(4,1)S(1)}, s32[]{:S(2)}) async-start(s8[5767168]{0:T(1024)(128)(4,1)} %bitcast.51), calls=%async_computation.8 | async-start | bytes 8388608
  454.1 10.7 %slice-start.1 = ((s8[5767168]{0:T(1024)(128)(4,1)}), s8[1572864]{0:T(1024)(128)(4,1)S(1)}, s32[]{:S(2)}) async-start(s8[5767168]{0:T(1024)(128)(4,1)} %bitcast.51), calls=%async_computation.9 | async-start | bytes 3145728
  454.1 10.6 %collective-permute-start.3 = (bf16[2,2816]{1,0:T(2,128)(2,1)S(1)}, bf16[2,2816]{1,0:T(2,128)(2,1)S(1)}, u32[]{:S(2)}, u32[]{:S(2)}) collective-permute-start(bf16[2,2816]{1,0:T(2,128)(2,1)S(1)} %slice.105), channel_id=1, source_target_pairs={{0,2},{2,4},{4,6},{6,8},{8,10},{10,12},{12,14},{14,16},{16,18},{18... | collective-permute-start | bytes 33800 | tf_op jit(solution)/shard_map/ppermute | solution.py:13
Sparse Core Ops, SparseCore 0:
  19.0 69.4 all-gather.6
  96.1 56.7 all-gather.8
  155.2 93.9 all-gather.12
  251.3 92.3 all-gather.10
  345.9 92.2 all-gather.14
  515.8 53.5 reduce-scatter.1
